TPU v7x, 256 devices: a whole 4x4x8 slice. The times are simulated.
256 devices in a mesh: sp: 16 (over y, x), tp: 16 (over z, core).
Axes of the slice: x: 4, y: 4, z: 8, core: 2. Of those that a mesh axis runs over, the one named last changes fastest.
Arguments:
- tokens: bfloat16 [8192, 2048], P(('sp', 'tp')), may hold values from -6 to 6
- query_vectors: bfloat16 [8192, 2048], P('sp', 'tp'), may hold values from -8 to 8
- key_vectors: bfloat16 [8192, 2048], P('sp', 'tp'), may hold values from -8 to 8
- value_vectors: bfloat16 [8192, 2048], P('sp', 'tp'), may hold values from -24 to 24
- cum_gate: float32 [8192, 32], P('sp', 'tp'), may hold values from -1028 to 0, as said below
- out_weight: bfloat16 [2048, 2048], P('tp'), may hold values from -0.125 to 0.125
- norm_gain: float32 [2048], replicated, may hold values from 0.1 to 1.9
- gate_weight: bfloat16 [16, 2048, 7168], P('sp', None, 'tp'), may hold values from -0.125 to 0.125
- up_weight: bfloat16 [16, 2048, 7168], P('sp', None, 'tp'), may hold values from -0.125 to 0.125
- down_weight: bfloat16 [16, 7168, 2048], P('sp', 'tp'), may hold values from -0.0625 to 0.0625
- expert_ids: int32 [8192, 2], P(('sp', 'tp')), may hold values from 0 to 15, all different within a row; in each aligned block of 32 rows (0 to 31, 32 to 63, ...) at most 6 rows name the same one
- route_weights: float32 [8192, 2], P(('sp', 'tp')), may hold values from 0.2 to 1
Outputs:
- layer_output: bfloat16 [8192, 2048], P(('sp', 'tp'))
Inputs may be any that keep to these rules, and one draw needn't show every extreme that they name: `cum_gate`: along the positions each head's values never rise. `expert_ids`: within the rows of one device no expert is named by more than 6 rows, and in some devices' rows one expert is named by exactly 6; a row names 2 different experts.
All inputs are finite; a program needn't handle non-finite values.
Results may differ from a plain program's by a relative error of at most 0.014.
Values may be sent and summed in bfloat16 or wider, within the bound.
A program may use at most 128 MiB of HBM per device.

v0:
```python
import math
import jax
import jax.numpy as jnp
from jax import lax
from jax.sharding import PartitionSpec as P

NEG_LARGE = -1e30


def copy_for_each(shard, axis):
    peers = lax.axis_size(axis)
    return lax.all_to_all(
        jnp.broadcast_to(shard[None], (peers, *shard.shape)), axis, 0, 0, tiled=True
    )


def in_order(parts, dim):
    parts = jnp.moveaxis(parts, 0, dim)
    dims = parts.shape
    return parts.reshape(*dims[:dim], dims[dim] * dims[dim + 1], *dims[dim + 2 :])


def collect(shard, axis, dim):
    parts = copy_for_each(shard, axis)
    return in_order(parts, dim)


def sent_together(arrays, axis, dim, along):
    widths = [a.shape[along] for a in arrays]
    both = jnp.concatenate(arrays, axis=along)
    filled = lax.all_gather(both, axis, axis=dim, tiled=True)
    return tuple(jnp.split(filled, [sum(widths[:k]) for k in range(1, len(widths))], axis=along))


def shards(
    tokens,
    query_vectors,
    key_vectors,
    value_vectors,
    cum_gate,
    out_weight,
    norm_gain,
    gate_weight,
    up_weight,
    down_weight,
    expert_ids,
    route_weights,
):
    sp_count = lax.axis_size("sp")
    seg_rows = query_vectors.shape[0]
    heads_here = cum_gate.shape[1]
    head_width = query_vectors.shape[1] // heads_here
    score_scale = head_width ** (-0.5)
    offset = lax.axis_index("sp") * seg_rows
    last_query = offset + seg_rows - 1
    query_pos = offset + jnp.arange(seg_rows, dtype=jnp.int32)
    query_heads = query_vectors.reshape(seg_rows, heads_here, head_width)
    query_gate = cum_gate.T
    gate_rows = collect(cum_gate, "sp", 0)

    def attend_block(carried, key_block, value_block, block_start):
        running_peak, running_total, accumulated = carried
        row_count = key_block.shape[0]
        key_heads = key_block.reshape(row_count, heads_here, head_width)
        value_heads = value_block.reshape(row_count, heads_here, head_width)
        key_gate = lax.dynamic_slice_in_dim(gate_rows, block_start, row_count, 0).T
        scores = (
            jnp.einsum("qhd,khd->hqk", query_heads, key_heads, preferred_element_type=jnp.float32)
            * score_scale
        )
        scores = scores + query_gate[:, :, None] - key_gate[:, None, :]
        key_pos = block_start + jnp.arange(row_count, dtype=jnp.int32)
        visible = (key_pos[None, :] <= query_pos[:, None])[None]
        scores = jnp.where(visible, scores, NEG_LARGE)
        new_peak = jnp.maximum(running_peak, jnp.max(scores, axis=2))
        exponent = jnp.where(visible, jnp.exp(scores - new_peak[:, :, None]), 0.0)
        rescale = jnp.exp(running_peak - new_peak)
        running_total = running_total * rescale + jnp.sum(exponent, axis=2)
        weighted = jnp.einsum(
            "hqk,khd->hqd",
            exponent.astype(jnp.bfloat16),
            value_heads,
            preferred_element_type=jnp.float32,
        )
        accumulated = accumulated * rescale[:, :, None] + weighted
        return (new_peak, running_total, accumulated)

    start_state = (
        jnp.full((heads_here, seg_rows), NEG_LARGE, jnp.float32),
        jnp.zeros((heads_here, seg_rows), jnp.float32),
        jnp.zeros((heads_here, seg_rows, head_width), jnp.float32),
    )
    carried = start_state
    key_piece, value_piece = sent_together((key_vectors, value_vectors), "sp", 0, 1)
    row_count = key_piece.shape[0]
    block_rows = math.gcd(row_count, 1024)
    block_count = row_count // block_rows
    key_stack = key_piece.reshape(block_count, block_rows, key_piece.shape[1])
    value_stack = value_piece.reshape(block_count, block_rows, value_piece.shape[1])

    def step_block(state, inputs):
        key_block, value_block, block_index = inputs
        block_start = block_index * block_rows

        def take_block(inner):
            return attend_block(inner, key_block, value_block, block_start)

        def skip_block(inner):
            return inner

        return (lax.cond(block_start <= last_query, take_block, skip_block, state), None)

    carried, _ = lax.scan(
        step_block, carried, (key_stack, value_stack, jnp.arange(block_count, dtype=jnp.int32))
    )
    final_peak, final_total, accumulated = carried
    attended = (accumulated / final_total[:, :, None]).astype(jnp.bfloat16)
    attended = attended.transpose(1, 0, 2).reshape(seg_rows, heads_here * head_width)
    tok_dev = tokens.shape[0]
    model_width = tokens.shape[1]
    token_rows = lax.all_to_all(attended, "tp", split_axis=0, concat_axis=1, tiled=True)
    projected = jnp.dot(
        token_rows,
        lax.all_gather(out_weight, "tp", axis=0, tiled=True),
        preferred_element_type=jnp.float32,
    )
    stream_wide = (tokens.astype(jnp.float32) + projected).astype(jnp.bfloat16).astype(jnp.float32)
    inverse = lax.rsqrt(jnp.mean(stream_wide * stream_wide, axis=1, keepdims=True) + 1e-05)
    normed = (stream_wide * inverse * norm_gain[None, :]).astype(jnp.bfloat16)
    n_experts = gate_weight.shape[0] * sp_count
    top_count = expert_ids.shape[1]
    capacity = max(2, 3 * tok_dev * top_count // (2 * n_experts))
    flat_ids = expert_ids.reshape(-1)
    hits = (flat_ids[:, None] == jnp.arange(n_experts, dtype=jnp.int32)[None, :]).astype(jnp.int32)
    earlier = jnp.cumsum(hits, axis=0) - hits
    slot_index = flat_ids * capacity + jnp.sum(earlier * hits, axis=1)
    placement_map = (
        jnp.arange(n_experts * capacity, dtype=jnp.int32)[:, None] == slot_index[None, :]
    ).astype(jnp.bfloat16)
    repeated = jnp.repeat(normed, top_count, axis=0)
    dispatch = jnp.dot(placement_map, repeated, preferred_element_type=jnp.float32).astype(
        jnp.bfloat16
    )
    dispatch = dispatch.reshape(n_experts, capacity, model_width)
    arrived = lax.all_to_all(dispatch, "sp", split_axis=0, concat_axis=0, tiled=True)
    row_block = arrived.reshape(-1, model_width)
    rows_in = lax.all_gather(row_block, "tp", axis=0, tiled=True)
    gate_value = jnp.dot(rows_in, gate_weight[0], preferred_element_type=jnp.float32)
    up_value = jnp.dot(rows_in, up_weight[0], preferred_element_type=jnp.float32)
    hidden = (jax.nn.silu(gate_value) * up_value).astype(jnp.bfloat16)
    summed = lax.psum_scatter(
        jnp.dot(hidden, down_weight[0], preferred_element_type=jnp.float32).astype(jnp.bfloat16),
        "tp",
        scatter_dimension=0,
        tiled=True,
    )
    returned = summed.reshape(arrived.shape)
    back = lax.all_to_all(returned, "sp", split_axis=0, concat_axis=0, tiled=True)
    flat_back = back.reshape(n_experts * capacity, model_width)
    picked = flat_back[slot_index].astype(jnp.float32).reshape(tok_dev, top_count, model_width)
    mixture = jnp.sum(picked * route_weights[:, :, None], axis=1)
    return (stream_wide + mixture).astype(jnp.bfloat16)


def solution(mesh):
    in_specs = (
        P(("sp", "tp"), None),
        P("sp", "tp"),
        P("sp", "tp"),
        P("sp", "tp"),
        P("sp", "tp"),
        P("tp", None),
        P(),
        P("sp", None, "tp"),
        P("sp", None, "tp"),
        P("sp", "tp", None),
        P(("sp", "tp"), None),
        P(("sp", "tp"), None),
    )
    out_specs = P(("sp", "tp"), None)
    return jax.shard_map(shards, mesh=mesh, in_specs=in_specs, out_specs=out_specs, check_vma=False)
```

profile of v0, /device:TPU:2, one launch (start us, length us, event | category | flops | bytes accessed | tf_op | source)
XLA Modules:
  0.0 335.4 jit_solution(8175806650671181984)
XLA Ops:
  6.5 1.8 pad_maximum_fusion
  8.4 0.7 all-gather.6.cloned.1.call-update
  9.2 1.3 broadcast_in_dim.61
  10.5 7.5 %all-to-all-start = ((f32[16,512,2]{1,2,0:T(2,128)}), f32[16,512,2]{1,2,0:T(2,128)S(1)}, u32[]{:S(2)}, u32[]{:S(2)}) async-start(f32[16,512,2]{1,2,0:T(2,128)} %broadcast_in_dim.61), calls=%async_computation | async-start | bytes 131072 | tf_op jit(solution)/shard_map/all_to_all | solution.py:12
  18.0 1.0 copy.28
  19.0 0.8 copy.33
  20.0 49.1 %all-gather.4.cloned.1.call-done = bf16[8192,256]{1,0:T(8,128)(2,1)} async-done(((bf16[512,256]{1,0:T(8,128)(2,1)}), bf16[8192,256]{1,0:T(8,128)(2,1)}) %all-gather.4.cloned.1.call-update) | async-done | bytes 4194320 | tf_op jit(solution)/shard_map/all_gather | solution.py:31
  69.2 4.4 %fusion.30 = (bf16[8192,128]{1,0:T(8,128)(2,1)}, bf16[8192,128]{1,0:T(8,128)(2,1)}) fusion(bf16[8192,256]{1,0:T(8,128)(2,1)} %all-gather.4.cloned.1.call-done), kind=kLoop, calls=%fused_computation.54 | loop fusion | bytes 8388608 | tf_op jit(solution)/shard_map/split | solution.py:32
  73.6 3.9 %copy.29 = bf16[8,1024,128]{1,2,0:T(8,128)(2,1)} copy(bf16[8,1024,128]{2,1,0:T(8,128)(2,1)} %bitcast.60) | data formatting | bytes 4194304
  77.5 3.9 %copy.30 = bf16[8,1024,128]{1,2,0:T(8,128)(2,1)} copy(bf16[8,1024,128]{2,1,0:T(8,128)(2,1)} %bitcast.59) | data formatting | bytes 4194304
  81.5 16.5 %while.15 = (s32[]{:T(128)}, f32[2,512]{1,0:T(2,128)S(1)}, f32[2,512]{1,0:T(2,128)S(1)}, f32[2,512,64]{1,2,0:T(8,128)S(1)}, s32[8]{0:T(128)S(1)}, /*index=5*/s32...) while((s32[]{:T(128)}, f32[2,512]{1,0:T(2,128)S(1)}, ...), condition=%wide.region_5.6_spmd.clone, body=%wide.region_0.5_spmd.clone.sunk | while | flops 289017344 | bytes 17043828 | solution.py:113
  81.5 0.6 dynamic_slice.31
  82.8 6.2 %conditional.3 = ((f32[2,512]{1,0:T(2,128)S(1)}, f32[2,512]{1,0:T(2,128)S(1)}, f32[2,512,64]{1,2,0:T(8,128)S(1)})) conditional(s32[]{:T(128)} %convert_element_type.83, (f32[2,512]{1,0:T(2,128)S(1)}, f32[2,512]{1,0:T(2,128)S(1)}, f32[2,512,64]{1,2,0:T(8,128)S(1)}) %tuple.43, (s32[]{:T(128)}, s32[]{:T(128)}, bf16[8,1024,128]{1,2,0:T(8,128)(2,1)}, ...), branch_computations={%region_1.1_spmd, %region_2.4_spmd} | conditional | flops 289017344 | bytes 17041490 | solution.py:111
  82.9 0.4 broadcast_compare_fusion
  83.3 1.1 constant_dynamic-slice_fusion
  84.3 1.4 fusion.4
  85.7 1.5 fusion.3
  87.2 1.7 fusion.8
  89.0 0.6 dynamic_slice.31
  90.3 0.6 dynamic_slice.31
  91.6 0.6 dynamic_slice.31
  92.9 0.6 dynamic_slice.31
  94.2 0.6 dynamic_slice.31
  95.5 0.6 dynamic_slice.31
  96.7 0.6 dynamic_slice.31
  98.1 0.2 copy.31
  98.2 0.8 all_to_all.24
  99.0 7.1 %all-to-all-start.1 = ((bf16[16,32,128]{2,1,0:T(8,128)(2,1)}), bf16[16,32,128]{2,1,0:T(8,128)(2,1)S(1)}, u32[]{:S(2)}, u32[]{:S(2)}) async-start(bf16[16,32,128]{2,1,0:T(8,128)(2,1)} %all_to_all.24), calls=%async_computation.1 | async-start | bytes 262144 | tf_op jit(solution)/shard_map/all_to_all | solution.py:121
  106.2 0.2 select_reduce_fusion
  106.4 10.4 %all-to-all-done.1 = bf16[16,32,128]{2,1,0:T(8,128)(2,1)S(1)} async-done(((bf16[16,32,128]{2,1,0:T(8,128)(2,1)}), bf16[16,32,128]{2,1,0:T(8,128)(2,1)S(1)}, u32[]{:S(2)}, u32[]{:S(2)}) %all-to-all-start.1) | async-done | bytes 131104 | tf_op jit(solution)/shard_map/all_to_all | solution.py:121
  116.8 12.6 %all-gather.6.cloned.1.call-done = bf16[2048,2048]{1,0:T(8,128)(2,1)} async-done(((bf16[128,2048]{1,0:T(8,128)(2,1)}), bf16[2048,2048]{1,0:T(8,128)(2,1)}) %all-gather.6.cloned.1.call-update) | async-done | bytes 8388624 | tf_op jit(solution)/shard_map/all_gather | solution.py:124
  129.4 5.0 %multiply_reduce_fusion.1 = (f32[32]{0:T(128)S(1)}, f32[32,2048]{1,0:T(8,128)S(1)}) fusion(bf16[2048,2048]{1,0:T(8,128)(2,1)} %all-gather.6.cloned.1.call-done, bf16[32,2048]{1,0:T(8,128)(2,1)S(1)} %copy-done.2, bf16[16,32,128]{2,1,0:T(8,128)(2,1)S(1)} %all-to-all-done.1), kind=kOutput, calls=%fused_computation.36 | convolution fusion | flops 268828640 | bytes 8913024 | tf_op jit(solution)/shard_map/dot_general | solution.py:122
  134.6 0.1 broadcast_in_dim.62
  134.9 0.2 convolution_convert_fusion.1
  135.2 44.9 %all_to_all.34 = bf16[16,6,2048]{2,1,0:T(8,128)(2,1)S(1)} all-to-all(bf16[16,6,2048]{2,1,0:T(8,128)(2,1)S(1)} %reshape.145), channel_id=1, replica_groups=mesh['sp'=16,'tp'=16] {'sp'}, dimensions={0} | all-to-all | bytes 786432 | tf_op jit(solution)/shard_map/all_to_all | solution.py:145
  180.1 0.9 reshape.146
  181.1 0.2 reduce-scatter.2.cloned.1.call-start
  181.3 40.0 %all-gather.8.cloned.1.call-done = bf16[1536,2048]{1,0:T(8,128)(2,1)} async-done(((bf16[96,2048]{1,0:T(8,128)(2,1)}), bf16[1536,2048]{1,0:T(8,128)(2,1)}) %all-gather.8.cloned.1.call-update) | async-done | bytes 6291472 | tf_op jit(solution)/shard_map/all_gather | solution.py:147
  221.2 7.9 %fusion.19 = f32[1536,448]{0,1:T(8,128)} fusion(bf16[1536,2048]{1,0:T(8,128)(2,1)} %all-gather.8.cloned.1.call-done, bf16[1,2048,448]{1,2,0:T(8,128)(2,1)} %param.23), kind=kOutput, calls=%fused_computation.30 | convolution fusion | flops 2818572288 | bytes 10878976 | tf_op jit(solution)/shard_map/dot_general | solution.py:148
  229.1 13.2 %convolution_convert_fusion = bf16[1536,2048]{1,0:T(8,128)(2,1)} fusion(bf16[1,448,2048]{2,1,0:T(8,128)(2,1)S(1)} %copy-done, bf16[1536,2048]{1,0:T(8,128)(2,1)} %all-gather.8.cloned.1.call-done, f32[1536,448]{0,1:T(8,128)} %fusion.19, bf16[1,2048,448]{1,2,0:T(8,128)(2,1)} %param.24), kind=kOutput, calls=%fused_computation.21 | convolution fusion | flops 5644419072 | bytes 19005440 | tf_op jit(solution)/shard_map/dot_general | solution.py:152
  242.3 65.9 %reduce-scatter.2.cloned.1.call-done = bf16[96,2048]{1,0:T(8,128)(2,1)} async-done(((bf16[1536,2048]{1,0:T(8,128)(2,1)}), bf16[96,2048]{1,0:T(8,128)(2,1)}) %reduce-scatter.2.cloned.1.call-update) | async-done | bytes 393232 | tf_op jit(solution)/shard_map/reduce_scatter | solution.py:151
  308.2 1.9 reshape.147
  310.2 7.2 %all-to-all-start.3 = ((bf16[16,6,2048]{2,1,0:T(8,128)(2,1)}), bf16[16,6,2048]{2,1,0:T(8,128)(2,1)S(1)}, u32[]{:S(2)}, u32[]{:S(2)}) async-start(bf16[16,6,2048]{2,1,0:T(8,128)(2,1)} %reshape.147), calls=%async_computation.4 | async-start | bytes 1048576 | tf_op jit(solution)/shard_map/all_to_all | solution.py:158
  317.7 8.5 %all-to-all-done.3 = bf16[16,6,2048]{2,1,0:T(8,128)(2,1)S(1)} async-done(((bf16[16,6,2048]{2,1,0:T(8,128)(2,1)}), bf16[16,6,2048]{2,1,0:T(8,128)(2,1)S(1)}, u32[]{:S(2)}, u32[]{:S(2)}) %all-to-all-start.3) | async-done | bytes 393248 | tf_op jit(solution)/shard_map/all_to_all | solution.py:158
  326.3 0.7 gather_fusion
  327.1 0.3 reshape.149
  327.4 0.7 multiply_reduce_fusion
  328.1 0.7 add_convert_fusion
  (60 shorter events, 1.5 us)
Async XLA Ops:
  6.5 222.6 %copy-start = (bf16[1,448,2048]{2,1,0:T(8,128)(2,1)S(1)}, bf16[1,448,2048]{2,1,0:T(8,128)(2,1)}, u32[]{:S(2)}) copy-start(bf16[1,448,2048]{2,1,0:T(8,128)(2,1)} %param.25) | copy-start | bytes 5505028
  6.5 62.6 %all-gather.4.cloned.1.call-start = ((), (), s32[]{:S(2)}) async-start(), calls=%async_computation.5 | async-start | bytes 4456448 | tf_op jit(solution)/shard_map/all_gather | solution.py:31
  8.4 121.0 %all-gather.6.cloned.1.call-start = ((), (), s32[]{:S(2)}) async-start(), calls=%async_computation.6 | async-start | bytes 8912896 | tf_op jit(solution)/shard_map/all_gather | solution.py:124
  10.5 70.9 %all-to-all-start = ((f32[16,512,2]{1,2,0:T(2,128)}), f32[16,512,2]{1,2,0:T(2,128)S(1)}, u32[]{:S(2)}, u32[]{:S(2)}) async-start(f32[16,512,2]{1,2,0:T(2,128)} %broadcast_in_dim.61), calls=%async_computation | async-start | bytes 131072 | tf_op jit(solution)/shard_map/all_to_all | solution.py:12
  73.6 7.9 %copy-start.1 = (f32[512,2]{0,1:T(2,128)S(1)}, f32[512,2]{0,1:T(2,128)}, u32[]{:S(2)}) copy-start(f32[512,2]{0,1:T(2,128)} %param.20) | copy-start | bytes 12292
  81.5 47.9 %copy-start.2 = (bf16[32,2048]{1,0:T(8,128)(2,1)S(1)}, bf16[32,2048]{1,0:T(8,128)(2,1)}, u32[]{:S(2)}) copy-start(bf16[32,2048]{1,0:T(8,128)(2,1)} %param.16) | copy-start | bytes 393220
  99.0 17.7 %all-to-all-start.1 = ((bf16[16,32,128]{2,1,0:T(8,128)(2,1)}), bf16[16,32,128]{2,1,0:T(8,128)(2,1)S(1)}, u32[]{:S(2)}, u32[]{:S(2)}) async-start(bf16[16,32,128]{2,1,0:T(8,128)(2,1)} %all_to_all.24), calls=%async_computation.1 | async-start | bytes 262144 | tf_op jit(solution)/shard_map/all_to_all | solution.py:121
  106.1 115.1 %all-gather.8.cloned.1.call-start = ((), (), s32[]{:S(2)}) async-start(), calls=%async_computation.7 | async-start | bytes 6684672 | tf_op jit(solution)/shard_map/all_gather | solution.py:147
  106.4 28.1 %copy-start.3 = (f32[2048]{0:T(1024)S(1)}, f32[2048]{0:T(1024)}, u32[]{:S(2)}) copy-start(f32[2048]{0:T(1024)} %param.22) | copy-start | bytes 24580
  181.1 127.2 %reduce-scatter.2.cloned.1.call-start = ((), (), s32[]{:S(2)}) async-start(), calls=%async_computation.8 | async-start | bytes 6684672 | tf_op jit(solution)/shard_map/reduce_scatter | solution.py:151
  242.3 75.1 %copy-start.4 = (s32[32,2]{0,1:T(2,128)S(1)}, s32[32,2]{0,1:T(2,128)}, u32[]{:S(2)}) copy-start(s32[32,2]{0,1:T(2,128)} %param.26) | copy-start | bytes 772
  242.3 75.3 %copy-start.5 = (f32[32,2]{0,1:T(2,128)S(1)}, f32[32,2]{0,1:T(2,128)}, u32[]{:S(2)}) copy-start(f32[32,2]{0,1:T(2,128)} %param.27) | copy-start | bytes 772
  310.2 16.0 %all-to-all-start.3 = ((bf16[16,6,2048]{2,1,0:T(8,128)(2,1)}), bf16[16,6,2048]{2,1,0:T(8,128)(2,1)S(1)}, u32[]{:S(2)}, u32[]{:S(2)}) async-start(bf16[16,6,2048]{2,1,0:T(8,128)(2,1)} %reshape.147), calls=%async_computation.4 | async-start | bytes 1048576 | tf_op jit(solution)/shard_map/all_to_all | solution.py:158
Sparse Core Ops, SparseCore 0:
  9.8 59.3 all-gather.3
  71.0 58.3 all-gather.5
  181.2 40.0 all-gather.7
  242.5 65.7 reduce-scatter.1
where the time goes:
time: 336 us; the launch traced here: 335 us
  waiting for transfers between devices  187 us (56%)
  blocking collectives  44.9 us (13%)
  matrix products  29.4 us (9%)
  local copies, waits for them, and re-layouts  27.1 us (8%)
  starting transfers between devices  22.1 us (7%)
  between operations  13.3 us (4%)
  loops' own time  5.68 us (2%)
  other arithmetic  5.62 us (2%)
    reduce_scatter x1, waiting for transfers between devices, shards(): lax.psum_scatter(jnp.dot(hidden, down_weight[0], preferred_element_type=j...  65.9 us
    all_gather x1, waiting for transfers between devices, sent_together(): filled = lax.all_gather(both, axis, axis=dim, tiled=True)  49.1 us
    all_to_all x1, blocking collectives, shards(): lax.all_to_all(dispatch, 'sp', split_axis=0, concat_axis=0, tiled=True)  44.9 us
    all_gather x1, waiting for transfers between devices, shards(): rows_in = lax.all_gather(row_block, 'tp', axis=0, tiled=True)  40 us
    dot_general x1, matrix products, shards(): jnp.dot(hidden, down_weight[0], preferred_element_type=jnp.float32)  13.2 us
    all_gather x1, waiting for transfers between devices, shards(): lax.all_gather(out_weight, 'tp', axis=0, tiled=True)  12.6 us
    all_to_all x1, waiting for transfers between devices, shards(): lax.all_to_all(attended, 'tp', split_axis=0, concat_axis=1, tiled=True)  10.4 us
    unnamed x17, local copies, waits for them, and re-layouts  9.73 us
  transfers between devices with their start and end apart: 7, of which 6 were waited for; matrix products, arithmetic and copies ran while one was open for 8% of the time, Pallas kernels for 0%

commit v1 on v0

--- a/solution.py
+++ b/solution.py
@@ -144,7 +144,9 @@
     dispatch = dispatch.reshape(n_experts, capacity, model_width)
     arrived = lax.all_to_all(dispatch, "sp", split_axis=0, concat_axis=0, tiled=True)
     row_block = arrived.reshape(-1, model_width)
-    rows_in = lax.all_gather(row_block, "tp", axis=0, tiled=True)
+    rows_in = jnp.concatenate(
+        lax.all_to_all(jnp.stack([row_block] * lax.axis_size("tp")), "tp", 0, 0), axis=0
+    )
     gate_value = jnp.dot(rows_in, gate_weight[0], preferred_element_type=jnp.float32)
     up_value = jnp.dot(rows_in, up_weight[0], preferred_element_type=jnp.float32)
     hidden = (jax.nn.silu(gate_value) * up_value).astype(jnp.bfloat16)

time: 336 us -> 435 us (1.29)
  blocking collectives: 44.9 us -> 187 us
  waiting for transfers between devices: 187 us -> 144 us
    all_to_all x0 -> x1, blocking collectives: none -> 142 us  [shards(): lax.all_to_all(jnp.stack([row_block] * lax.axis_size('tp')), 'tp', 0, 0)]
    all_gather x1 -> x0, waiting for transfers between devices: 40 us -> none  [shards(): rows_in = lax.all_gather(row_block, 'tp', axis=0, tiled=True)]
    unnamed x17 -> x21, local copies, waits for them, and re-layouts: 9.73 us -> 12.4 us
  transfers between devices with their start and end apart: 7 -> 6, of which waited for: 6 -> 5; matrix products, arithmetic and copies ran while one was open for 8% -> 6% of each run, Pallas kernels for 0% -> 0%
where the time goes in v1:
time: 435 us; the launch traced here: 434 us
  blocking collectives  187 us (43%)
  waiting for transfers between devices  144 us (33%)
  local copies, waits for them, and re-layouts  29.7 us (7%)
  matrix products  26.1 us (6%)
  starting transfers between devices  21.8 us (5%)
  between operations  13.3 us (3%)
  loops' own time  5.68 us (1%)
  other arithmetic  5.62 us (1%)
    all_to_all x1, blocking collectives, shards(): lax.all_to_all(jnp.stack([row_block] * lax.axis_size('tp')), 'tp', 0, 0)  142 us
    reduce_scatter x1, waiting for transfers between devices, shards(): lax.psum_scatter(jnp.dot(hidden, down_weight[0], preferred_element_type=j...  63.1 us
    all_gather x1, waiting for transfers between devices, sent_together(): filled = lax.all_gather(both, axis, axis=dim, tiled=True)  49.1 us
    all_to_all x1, blocking collectives, shards(): lax.all_to_all(dispatch, 'sp', split_axis=0, concat_axis=0, tiled=True)  44.9 us
    dot_general x1, matrix products, shards(): jnp.dot(hidden, down_weight[0], preferred_element_type=jnp.float32)  13.2 us
    all_gather x1, waiting for transfers between devices, shards(): lax.all_gather(out_weight, 'tp', axis=0, tiled=True)  12.6 us
    unnamed x21, local copies, waits for them, and re-layouts  12.4 us
    all_to_all x1, waiting for transfers between devices, shards(): lax.all_to_all(attended, 'tp', split_axis=0, concat_axis=1, tiled=True)  10.4 us
  transfers between devices with their start and end apart: 6, of which 5 were waited for; matrix products, arithmetic and copies ran while one was open for 6% of the time, Pallas kernels for 0%

profile of v1, /device:TPU:2, one launch (start us, length us, event | category | flops | bytes accessed | tf_op | source)
XLA Modules:
  0.0 433.9 jit_solution(18144878411443872926)
XLA Ops:
  6.5 1.8 pad_maximum_fusion
  8.5 0.7 all-gather.5.cloned.1.call-update
  9.2 1.3 broadcast_in_dim.61
  10.5 7.5 %all-to-all-start = ((f32[16,512,2]{1,2,0:T(2,128)}), f32[16,512,2]{1,2,0:T(2,128)S(1)}, u32[]{:S(2)}, u32[]{:S(2)}) async-start(f32[16,512,2]{1,2,0:T(2,128)} %broadcast_in_dim.61), calls=%async_computation | async-start | bytes 131072 | tf_op jit(solution)/shard_map/all_to_all | solution.py:12
  18.0 1.0 copy.28
  19.0 0.8 copy.33
  20.0 49.1 %all-gather.3.cloned.1.call-done = bf16[8192,256]{1,0:T(8,128)(2,1)} async-done(((bf16[512,256]{1,0:T(8,128)(2,1)}), bf16[8192,256]{1,0:T(8,128)(2,1)}) %all-gather.3.cloned.1.call-update) | async-done | bytes 4194320 | tf_op jit(solution)/shard_map/all_gather | solution.py:31
  69.2 4.4 %fusion.30 = (bf16[8192,128]{1,0:T(8,128)(2,1)}, bf16[8192,128]{1,0:T(8,128)(2,1)}) fusion(bf16[8192,256]{1,0:T(8,128)(2,1)} %all-gather.3.cloned.1.call-done), kind=kLoop, calls=%fused_computation.54 | loop fusion | bytes 8388608 | tf_op jit(solution)/shard_map/split | solution.py:32
  73.6 3.9 copy.29
  77.5 3.9 copy.30
  81.5 16.5 %while.15 = (s32[]{:T(128)}, f32[2,512]{1,0:T(2,128)S(1)}, f32[2,512]{1,0:T(2,128)S(1)}, f32[2,512,64]{1,2,0:T(8,128)S(1)}, s32[8]{0:T(128)S(1)}, /*index=5*/s32...) while((s32[]{:T(128)}, f32[2,512]{1,0:T(2,128)S(1)}, ...), condition=%wide.region_5.6_spmd.clone, body=%wide.region_0.5_spmd.clone.sunk | while | flops 289017344 | bytes 17043828 | solution.py:113
  81.5 0.6 dynamic_slice.31
  82.8 6.2 %conditional.3 = ((f32[2,512]{1,0:T(2,128)S(1)}, f32[2,512]{1,0:T(2,128)S(1)}, f32[2,512,64]{1,2,0:T(8,128)S(1)})) conditional(s32[]{:T(128)} %convert_element_type.83, (f32[2,512]{1,0:T(2,128)S(1)}, f32[2,512]{1,0:T(2,128)S(1)}, f32[2,512,64]{1,2,0:T(8,128)S(1)}) %tuple.43, (s32[]{:T(128)}, s32[]{:T(128)}, bf16[8,1024,128]{1,2,0:T(8,128)(2,1)}, ...), branch_computations={%region_1.1_spmd, %region_2.4_spmd} | conditional | flops 289017344 | bytes 17041490 | solution.py:111
  82.9 0.4 broadcast_compare_fusion
  83.3 1.1 constant_dynamic-slice_fusion
  84.3 1.4 fusion.4
  85.7 1.5 fusion.3
  87.2 1.7 fusion.8
  89.0 0.6 dynamic_slice.31
  90.3 0.6 dynamic_slice.31
  91.6 0.6 dynamic_slice.31
  92.8 0.6 dynamic_slice.31
  94.1 0.6 dynamic_slice.31
  95.4 0.6 dynamic_slice.31
  96.7 0.6 dynamic_slice.31
  98.0 0.2 copy.31
  98.2 0.8 all_to_all.27
  99.0 7.1 %all-to-all-start.1 = ((bf16[16,32,128]{2,1,0:T(8,128)(2,1)}), bf16[16,32,128]{2,1,0:T(8,128)(2,1)S(1)}, u32[]{:S(2)}, u32[]{:S(2)}) async-start(bf16[16,32,128]{2,1,0:T(8,128)(2,1)} %all_to_all.27), calls=%async_computation.1 | async-start | bytes 262144 | tf_op jit(solution)/shard_map/all_to_all | solution.py:121
  106.2 0.2 select_reduce_fusion
  106.4 10.4 %all-to-all-done.1 = bf16[16,32,128]{2,1,0:T(8,128)(2,1)S(1)} async-done(((bf16[16,32,128]{2,1,0:T(8,128)(2,1)}), bf16[16,32,128]{2,1,0:T(8,128)(2,1)S(1)}, u32[]{:S(2)}, u32[]{:S(2)}) %all-to-all-start.1) | async-done | bytes 131104 | tf_op jit(solution)/shard_map/all_to_all | solution.py:121
  116.8 12.6 %all-gather.5.cloned.1.call-done = bf16[2048,2048]{1,0:T(8,128)(2,1)} async-done(((bf16[128,2048]{1,0:T(8,128)(2,1)}), bf16[2048,2048]{1,0:T(8,128)(2,1)}) %all-gather.5.cloned.1.call-update) | async-done | bytes 8388624 | tf_op jit(solution)/shard_map/all_gather | solution.py:124
  129.4 5.0 %multiply_reduce_fusion.1 = (f32[32]{0:T(128)S(1)}, f32[32,2048]{1,0:T(8,128)S(1)}) fusion(bf16[2048,2048]{1,0:T(8,128)(2,1)} %all-gather.5.cloned.1.call-done, bf16[32,2048]{1,0:T(8,128)(2,1)S(1)} %copy-done.3, bf16[16,32,128]{2,1,0:T(8,128)(2,1)S(1)} %all-to-all-done.1), kind=kOutput, calls=%fused_computation.36 | convolution fusion | flops 268828640 | bytes 8913024 | tf_op jit(solution)/shard_map/dot_general | solution.py:122
  134.6 0.1 broadcast_in_dim.62
  134.9 0.2 convolution_convert_fusion.1
  135.2 44.9 %all_to_all.39 = bf16[16,6,2048]{2,1,0:T(8,128)(2,1)S(1)} all-to-all(bf16[16,6,2048]{2,1,0:T(8,128)(2,1)S(1)} %reshape.147), channel_id=1, replica_groups=mesh['sp'=16,'tp'=16] {'sp'}, dimensions={0} | all-to-all | bytes 786432 | tf_op jit(solution)/shard_map/all_to_all | solution.py:145
  180.2 0.8 stack.3
  181.1 142.3 %all_to_all.40 = bf16[16,96,2048]{2,1,0:T(8,128)(2,1)S(1)} all-to-all(bf16[16,96,2048]{2,1,0:T(8,128)(2,1)S(1)} %stack.3), channel_id=1, replica_groups=mesh['sp'=16,'tp'=16] {'tp'}, dimensions={0} | all-to-all | bytes 12582912 | tf_op jit(solution)/shard_map/all_to_all | solution.py:148
  323.4 2.7 copy-done.1
  326.0 4.6 %fusion.19 = f32[1536,448]{0,1:T(8,128)} fusion(bf16[1536,2048]{1,0:T(8,128)(2,1)S(1)} %bitcast.64, bf16[1,2048,448]{1,2,0:T(8,128)(2,1)S(1)} %copy-done.7), kind=kOutput, calls=%fused_computation.30 | convolution fusion | flops 2818572288 | bytes 10878976 | tf_op jit(solution)/shard_map/dot_general | solution.py:150
  330.6 13.2 %convolution_convert_fusion = bf16[1536,2048]{1,0:T(8,128)(2,1)} fusion(bf16[1,448,2048]{2,1,0:T(8,128)(2,1)S(1)} %copy-done, bf16[1536,2048]{1,0:T(8,128)(2,1)} %bitcast.65, f32[1536,448]{0,1:T(8,128)} %fusion.19, bf16[1,2048,448]{1,2,0:T(8,128)(2,1)} %param.24), kind=kOutput, calls=%fused_computation.21 | convolution fusion | flops 5644419072 | bytes 19005440 | tf_op jit(solution)/shard_map/dot_general | solution.py:154
  343.9 63.1 %reduce-scatter.2.cloned.1.call-done = bf16[96,2048]{1,0:T(8,128)(2,1)} async-done(((bf16[1536,2048]{1,0:T(8,128)(2,1)}), bf16[96,2048]{1,0:T(8,128)(2,1)}) %reduce-scatter.2.cloned.1.call-update) | async-done | bytes 393232 | tf_op jit(solution)/shard_map/reduce_scatter | solution.py:153
  406.9 1.9 reshape.149
  408.8 7.1 %all-to-all-start.4 = ((bf16[16,6,2048]{2,1,0:T(8,128)(2,1)}), bf16[16,6,2048]{2,1,0:T(8,128)(2,1)S(1)}, u32[]{:S(2)}, u32[]{:S(2)}) async-start(bf16[16,6,2048]{2,1,0:T(8,128)(2,1)} %reshape.149), calls=%async_computation.5 | async-start | bytes 1048576 | tf_op jit(solution)/shard_map/all_to_all | solution.py:160
  416.3 8.5 %all-to-all-done.4 = bf16[16,6,2048]{2,1,0:T(8,128)(2,1)S(1)} async-done(((bf16[16,6,2048]{2,1,0:T(8,128)(2,1)}), bf16[16,6,2048]{2,1,0:T(8,128)(2,1)S(1)}, u32[]{:S(2)}, u32[]{:S(2)}) %all-to-all-start.4) | async-done | bytes 393248 | tf_op jit(solution)/shard_map/all_to_all | solution.py:160
  424.9 0.7 gather_fusion
  425.6 0.3 reshape.151
  425.9 0.7 multiply_reduce_fusion
  426.7 0.7 add_convert_fusion
  (63 shorter events, 1.6 us)
Async XLA Ops:
  6.5 324.1 %copy-start = (bf16[1,448,2048]{2,1,0:T(8,128)(2,1)S(1)}, bf16[1,448,2048]{2,1,0:T(8,128)(2,1)}, u32[]{:S(2)}) copy-start(bf16[1,448,2048]{2,1,0:T(8,128)(2,1)} %param.25) | copy-start | bytes 5505028
  6.5 62.6 %all-gather.3.cloned.1.call-start = ((), (), s32[]{:S(2)}) async-start(), calls=%async_computation.6 | async-start | bytes 4456448 | tf_op jit(solution)/shard_map/all_gather | solution.py:31
  8.4 121.0 %all-gather.5.cloned.1.call-start = ((), (), s32[]{:S(2)}) async-start(), calls=%async_computation.7 | async-start | bytes 8912896 | tf_op jit(solution)/shard_map/all_gather | solution.py:124
  10.5 70.9 %all-to-all-start = ((f32[16,512,2]{1,2,0:T(2,128)}), f32[16,512,2]{1,2,0:T(2,128)S(1)}, u32[]{:S(2)}, u32[]{:S(2)}) async-start(f32[16,512,2]{1,2,0:T(2,128)} %broadcast_in_dim.61), calls=%async_computation | async-start | bytes 131072 | tf_op jit(solution)/shard_map/all_to_all | solution.py:12
  73.6 7.9 %copy-start.2 = (f32[512,2]{0,1:T(2,128)S(1)}, f32[512,2]{0,1:T(2,128)}, u32[]{:S(2)}) copy-start(f32[512,2]{0,1:T(2,128)} %param.20) | copy-start | bytes 12292
  81.5 47.9 %copy-start.3 = (bf16[32,2048]{1,0:T(8,128)(2,1)S(1)}, bf16[32,2048]{1,0:T(8,128)(2,1)}, u32[]{:S(2)}) copy-start(bf16[32,2048]{1,0:T(8,128)(2,1)} %param.16) | copy-start | bytes 393220
  99.0 17.8 %all-to-all-start.1 = ((bf16[16,32,128]{2,1,0:T(8,128)(2,1)}), bf16[16,32,128]{2,1,0:T(8,128)(2,1)S(1)}, u32[]{:S(2)}, u32[]{:S(2)}) async-start(bf16[16,32,128]{2,1,0:T(8,128)(2,1)} %all_to_all.27), calls=%async_computation.1 | async-start | bytes 262144 | tf_op jit(solution)/shard_map/all_to_all | solution.py:121
  106.1 300.8 %reduce-scatter.2.cloned.1.call-start = ((), (), s32[]{:S(2)}) async-start(), calls=%async_computation.8 | async-start | bytes 6684672 | tf_op jit(solution)/shard_map/reduce_scatter | solution.py:153
  106.4 28.1 %copy-start.4 = (f32[2048]{0:T(1024)S(1)}, f32[2048]{0:T(1024)}, u32[]{:S(2)}) copy-start(f32[2048]{0:T(1024)} %param.22) | copy-start | bytes 24580
  181.1 145.0 %copy-start.7 = (bf16[1,2048,448]{1,2,0:T(8,128)(2,1)S(1)}, bf16[1,2048,448]{1,2,0:T(8,128)(2,1)}, u32[]{:S(2)}) copy-start(bf16[1,2048,448]{1,2,0:T(8,128)(2,1)} %param.23) | copy-start | bytes 5505028
  323.4 2.7 copy-start.1
  343.8 72.1 %copy-start.5 = (s32[32,2]{0,1:T(2,128)S(1)}, s32[32,2]{0,1:T(2,128)}, u32[]{:S(2)}) copy-start(s32[32,2]{0,1:T(2,128)} %param.26) | copy-start | bytes 772
  343.8 72.3 %copy-start.6 = (f32[32,2]{0,1:T(2,128)S(1)}, f32[32,2]{0,1:T(2,128)}, u32[]{:S(2)}) copy-start(f32[32,2]{0,1:T(2,128)} %param.27) | copy-start | bytes 772
  408.8 15.9 %all-to-all-start.4 = ((bf16[16,6,2048]{2,1,0:T(8,128)(2,1)}), bf16[16,6,2048]{2,1,0:T(8,128)(2,1)S(1)}, u32[]{:S(2)}, u32[]{:S(2)}) async-start(bf16[16,6,2048]{2,1,0:T(8,128)(2,1)} %reshape.149), calls=%async_computation.5 | async-start | bytes 1048576 | tf_op jit(solution)/shard_map/all_to_all | solution.py:160
Sparse Core Ops, SparseCore 0:
  9.8 59.3 all-gather.2
  71.0 58.3 all-gather.4
  344.0 62.9 reduce-scatter.1
